TPU v7x, 32 devices: a whole 2x2x4 slice. The times are simulated.
32 devices in a mesh: tp: 8 (over z, y), dp: 4 (over x, core).
Axes of the slice: x: 2, y: 2, z: 4, core: 2. Of those that a mesh axis runs over, the one named last changes fastest.
Arguments:
- tokens: bfloat16 [96, 4096], P('tp', 'dp'), may hold values from -6 to 6
- lengths: int32 [24], P('dp'), may hold values from 1 to 4, 42 in all
- norm_gain: float32 [2, 4096], P(None, 'dp'), may hold values from 0.1 to 1.9
- gate_weight: bfloat16 [2, 4096, 8192], P(None, 'dp', 'tp'), may hold values from -0.09375 to 0.09375
- value_weight: bfloat16 [2, 4096, 8192], P(None, 'dp', 'tp'), may hold values from -0.09375 to 0.09375
- vector_weight: bfloat16 [2, 4096, 2, 2048], P(None, 'dp', None, 'tp'), may hold values from -0.09375 to 0.09375
- step_weight: bfloat16 [2, 4096, 128], P(None, 'dp'), may hold values from -0.09375 to 0.09375
- step_bias: float32 [2, 128], P(None, 'tp'), may hold values from -3 to 0
- decay_rate: float32 [2, 128], P(None, 'tp'), may hold values from 0.003 to 1
- value_taps: bfloat16 [2, 4, 8192], P(None, None, 'tp'), may hold values from -3 to 3
- vector_taps: bfloat16 [2, 4, 2, 2048], P(None, None, None, 'tp'), may hold values from -3 to 3
- out_weight: bfloat16 [2, 8192, 4096], P(None, 'tp', 'dp'), may hold values from -0.0625 to 0.0625
- recurrent_state: float32 [2, 24, 128, 64, 128], P(None, 'dp', 'tp'), may hold values from -4 to 4
- value_history: bfloat16 [2, 24, 3, 8192], P(None, 'dp', None, 'tp'), may hold values from -6 to 6
- vector_history: bfloat16 [2, 24, 3, 2, 2048], P(None, 'dp', None, None, 'tp'), may hold values from -6 to 6
Outputs:
- next_tokens: bfloat16 [96, 4096], P('tp', 'dp')
- next_state: float32 [2, 24, 128, 64, 128], P(None, 'dp', 'tp')
- next_value_history: bfloat16 [2, 24, 3, 8192], P(None, 'dp', None, 'tp')
- next_vector_history: bfloat16 [2, 24, 3, 2, 2048], P(None, 'dp', None, None, 'tp')
Inputs may be any that keep to these rules, and one draw needn't show every extreme that they name: `lengths`: the number of live new tokens of each sequence; some sequences have more than twice the mean.
All inputs are finite; a program needn't handle non-finite values. No bound on the sum of `lengths` on one device may be relied on, other than what follows from the above.
Results may differ from a plain program's by a relative error of at most 0.029.
Values may be sent and summed in bfloat16 or wider, within the bound.
A program may use at most 128 MiB of HBM per device.

v0:
```python
import jax
import jax.numpy as jnp
from jax import lax
from jax.sharding import PartitionSpec as P

D = 4096
HEADS = 128
HEAD_DIM = 64
STATE = 128
GROUPS = 16
CONV = 4
NEW = 4
LAYERS = 2


norm_floor = 0.1
highest = lax.Precision.HIGHEST


def short_conv(history, fresh_rows, conv_taps):
    padded = jnp.concatenate([history, fresh_rows], axis=1)
    block_len = fresh_rows.shape[1]
    summed = jnp.zeros(fresh_rows.shape, jnp.float32)
    for offset in range(conv_taps.shape[0]):
        summed = summed + padded[:, offset : offset + block_len].astype(jnp.float32) * conv_taps[
            offset
        ].astype(jnp.float32)
    return (jax.nn.silu(summed), padded)


def state_block(values, write_vec, read_vec, step_sizes, rate_vec, carried_state):
    block_len = values.shape[1]
    cumulative = jnp.cumsum(step_sizes * rate_vec, axis=1)
    causal = jnp.tril(jnp.ones((block_len, block_len), dtype=bool))[None, :, :, None, None]
    log_gap = cumulative[:, :, None] - cumulative[:, None, :]
    decays = jnp.where(causal, jnp.exp(-jnp.where(causal, log_gap, 0.0)), 0.0)
    scores = jnp.einsum("stgn,sugn->stug", read_vec, write_vec, precision=highest)
    weights = scores[..., None] * decays * step_sizes[:, None]
    within = jnp.einsum("stugr,sugrp->stgrp", weights, values, precision=highest)
    carried = (
        jnp.einsum("stgn,sgrpn->stgrp", read_vec, carried_state, precision=highest)
        * jnp.exp(-cumulative)[..., None]
    )
    ending = jnp.exp(cumulative - cumulative[:, -1:]) * step_sizes
    weighted = values * ending[..., None]
    fresh_state = jnp.einsum("sugrp,sugn->sgrpn", weighted, write_vec, precision=highest)
    next_state = carried_state * jnp.exp(-cumulative[:, -1])[..., None, None] + fresh_state
    return (within + carried, next_state)


def collect(token_rows):
    return lax.all_gather(token_rows, "tp", axis=0, tiled=True)


def body(
    tokens,
    lengths,
    norm_gain,
    gate_weight,
    value_weight,
    vector_weight,
    step_weight,
    step_bias,
    decay_rate,
    value_taps,
    vector_taps,
    out_weight,
    recurrent_state,
    value_history,
    vector_history,
):
    local_seqs = lengths.shape[0]
    local_heads = step_bias.shape[1]
    local_tokens = local_seqs * NEW
    heads_group = HEADS // GROUPS
    group_count = max(1, local_heads // heads_group)
    per_group = local_heads // group_count
    live_mask = (jnp.arange(NEW, dtype=jnp.int32)[None, :] < lengths[:, None]).astype(jnp.float32)
    kept_rows = lengths[:, None] + jnp.arange(CONV - 1, dtype=jnp.int32)[None, :]
    picker = (
        kept_rows[:, :, None] == jnp.arange(CONV - 1 + NEW, dtype=jnp.int32)[None, None, :]
    ).astype(jnp.bfloat16)
    head_start = lax.axis_index("tp") * local_heads
    first_group = head_start // heads_group
    token_rows = tokens
    whole = collect(tokens)
    state_list, value_list, vector_list = ([], [], [])
    for ordinal in range(LAYERS):
        widened = whole.astype(jnp.float32)
        squares = jnp.sum(widened * widened, axis=1)
        normed = (widened * norm_gain[ordinal]).astype(jnp.bfloat16)
        own_step = lax.dynamic_slice_in_dim(step_weight[ordinal], head_start, local_heads, 1)
        gate_part = jnp.dot(normed, gate_weight[ordinal], preferred_element_type=jnp.float32)
        value_part = jnp.dot(normed, value_weight[ordinal], preferred_element_type=jnp.float32)
        vector_part = jnp.einsum(
            "td,dkc->tkc", normed, vector_weight[ordinal], preferred_element_type=jnp.float32
        )
        step_part = jnp.dot(normed, own_step, preferred_element_type=jnp.float32)
        gate_sum, value_sum, vector_sum, step_sum, own_squares = (
            lax.psum_scatter(gate_part, "dp", scatter_dimension=0, tiled=True),
            lax.psum_scatter(value_part, "dp", scatter_dimension=0, tiled=True),
            lax.psum_scatter(vector_part, "dp", scatter_dimension=0, tiled=True),
            lax.psum_scatter(step_part, "dp", scatter_dimension=0, tiled=True),
            lax.psum_scatter(squares, "dp", scatter_dimension=0, tiled=True),
        )
        scaling = lax.rsqrt(own_squares / D + norm_floor)[:, None]
        gate = (gate_sum * scaling).astype(jnp.bfloat16)
        value_in = (value_sum * scaling).astype(jnp.bfloat16)
        vector_in = (vector_sum * scaling[:, :, None]).astype(jnp.bfloat16)
        step_in = (step_sum * scaling).astype(jnp.bfloat16)
        step_sizes = (
            jax.nn.softplus(
                step_in.astype(jnp.float32).reshape(local_seqs, NEW, local_heads)
                + step_bias[ordinal]
            )
            * live_mask[:, :, None]
        )
        value_conv, padded_value = short_conv(
            value_history[ordinal], value_in.reshape(local_seqs, NEW, -1), value_taps[ordinal]
        )
        vector_conv, padded_vector = short_conv(
            vector_history[ordinal], vector_in.reshape(local_seqs, NEW, 2, -1), vector_taps[ordinal]
        )
        vector_whole = lax.all_gather(vector_conv, "tp", axis=3, tiled=True)
        arranged = vector_whole.reshape(local_seqs, NEW, 2, STATE, GROUPS)
        own_vectors = lax.dynamic_slice_in_dim(arranged, first_group, group_count, 4)
        write_vec = jnp.swapaxes(own_vectors[:, :, 0], 2, 3)
        read_vec = jnp.swapaxes(own_vectors[:, :, 1], 2, 3)
        output, next_state = state_block(
            value_conv.reshape(local_seqs, NEW, group_count, per_group, HEAD_DIM),
            write_vec,
            read_vec,
            step_sizes.reshape(local_seqs, NEW, group_count, per_group),
            decay_rate[ordinal].reshape(group_count, per_group),
            recurrent_state[ordinal].reshape(local_seqs, group_count, per_group, HEAD_DIM, STATE),
        )
        state_list.append(next_state.reshape(recurrent_state.shape[1:]))
        value_list.append(
            jnp.einsum(
                "sjk,skc->sjc", picker, padded_value, preferred_element_type=jnp.float32
            ).astype(jnp.bfloat16)
        )
        vector_list.append(
            jnp.einsum(
                "sjk,skmc->sjmc", picker, padded_vector, preferred_element_type=jnp.float32
            ).astype(jnp.bfloat16)
        )
        gated = (
            output.reshape(local_seqs, NEW, -1)
            * jax.nn.silu(gate.astype(jnp.float32).reshape(local_seqs, NEW, -1))
            * live_mask[:, :, None]
        )
        mixed = gated.reshape(local_tokens, -1).astype(jnp.bfloat16)
        mixed_all = lax.all_gather(mixed, "dp", axis=0, tiled=True)
        layer_out = out_weight[ordinal]
        update = lax.psum_scatter(
            jnp.dot(mixed_all, layer_out, preferred_element_type=jnp.float32),
            "tp",
            scatter_dimension=0,
            tiled=True,
        )
        token_rows = (token_rows.astype(jnp.float32) + update).astype(jnp.bfloat16)
        if ordinal + 1 < LAYERS:
            whole = collect(token_rows)
    return (token_rows, jnp.stack(state_list), jnp.stack(value_list), jnp.stack(vector_list))


def solution(mesh):
    return jax.shard_map(
        body,
        mesh=mesh,
        in_specs=(
            P("tp", "dp"),
            P("dp"),
            P(None, "dp"),
            P(None, "dp", "tp"),
            P(None, "dp", "tp"),
            P(None, "dp", None, "tp"),
            P(None, "dp", None),
            P(None, "tp"),
            P(None, "tp"),
            P(None, None, "tp"),
            P(None, None, None, "tp"),
            P(None, "tp", "dp"),
            P(None, "dp", "tp", None, None),
            P(None, "dp", None, "tp"),
            P(None, "dp", None, None, "tp"),
        ),
        out_specs=(
            P("tp", "dp"),
            P(None, "dp", "tp", None, None),
            P(None, "dp", None, "tp"),
            P(None, "dp", None, None, "tp"),
        ),
        check_vma=False,
    )
```

profile of v0, /device:TPU:0, one launch (start us, length us, event | category | flops | bytes accessed | tf_op | source)
XLA Modules:
  0.0 362.8 jit_solution(17004689066168184645)
XLA Ops:
  8.0 32.8 %all-gather = bf16[8,12,1024]{2,1,0:T(8,128)(2,1)S(1)} all-gather(bf16[1,12,1024]{2,1,0:T(8,128)(2,1)} %bitcast.213), channel_id=1, replica_groups=mesh['tp'=8,'dp'=4] {'tp'}, dimensions={0}, use_global_device_ids=true | all-gather | bytes 221184 | tf_op jit(solution)/shard_map/all_gather | solution.py:52
  40.8 3.5 fusion.140
  45.5 2.9 fusion.12
  48.5 2.9 fusion.10
  55.9 5.9 %all-reduce.9 = (f32[96,16]{0,1:T(8,128)S(1)}, f32[96]{0:T(128)S(1)}) all-reduce(f32[96,16]{0,1:T(8,128)S(1)} %fusion.32, f32[96]{0:T(128)S(1)} %get-tuple-element.36), channel_id=5, replica_groups=mesh['tp'=8,'dp'=4] {'dp'}, use_global_device_ids=true, to_apply=%region_4.5.clone | all-reduce | flops 1632 | bytes 13056
  70.6 5.4 %fusion.139 = (f32[1,6,16,64,128]{4,3,2,1,0:T(8,128)}, f32[1,6,16,64,128]{4,3,2,1,0:T(8,128)S(1)}) fusion(f32[2,6,16,64,128]{4,3,2,1,0:T(8,128)} %param.27), kind=kLoop, calls=%fused_computation.246 | loop fusion | bytes 12582912 | tf_op jit(solution)/shard_map/slice | solution.py:135
  78.3 31.1 %all_gather.19 = f32[6,4,2,2048]{3,1,2,0:T(4,128)S(1)} all-gather(f32[6,4,2,256]{3,1,2,0:T(4,128)S(1)} %divide_multiply_fusion.3), channel_id=1, replica_groups=mesh['tp'=8,'dp'=4] {'tp'}, dimensions={3}, use_global_device_ids=true | all-gather | bytes 442368 | tf_op jit(solution)/shard_map/all_gather | solution.py:124
  112.2 4.4 %constant_dynamic-slice_fusion.1 = (f32[6,4,1,128,2]{4,3,1,2,0:T(8,128)}, f32[6,4,1,128,2]{4,3,1,2,0:T(8,128)}) fusion(f32[6,4,2,128,16]{4,3,1,2,0:T(8,128)} %reshape.307, s32[]{:T(128)S(6)} %select_n.55, s32[]{:T(128)S(6)} %add.254), kind=kLoop, calls=%fused_computation.216 | loop fusion | bytes 98312 | tf_op jit(solution)/shard_map/slice | solution.py:127
  121.5 10.0 %fusion.22 = f32[6,4,2,8,64]{4,1,3,2,0:T(4,128)} fusion(f32[6,2,8,64,128]{4,3,2,1,0:T(8,128)} %bitcast.209, f32[6,4,2,8]{1,3,2,0:T(8,128)S(1)} %copy-done.20, f32[6,4,1,128,2]{3,1,4,0,2:T(4,128)S(1)} %copy.138), kind=kOutput, calls=%fused_computation.27 | convolution fusion | flops 37773312 | bytes 3270144 | tf_op jit(solution)/shard_map/stgn,sgrpn->stgrp/dot_general | solution.py:41
  137.6 5.8 %all_gather.20 = bf16[96,1024]{1,0:T(8,128)(2,1)S(1)} all-gather(bf16[24,1024]{1,0:T(8,128)(2,1)S(1)} %fusion.81), channel_id=1, replica_groups=mesh['tp'=8,'dp'=4] {'dp'}, dimensions={0}, use_global_device_ids=true | all-gather | bytes 245760 | tf_op jit(solution)/shard_map/all_gather | solution.py:154
  146.3 25.5 %fusion = f32[16,1024]{1,0:T(8,128)S(1)} fusion(f32[96,1024]{1,0:T(8,128)} %fusion.8), kind=kCustom, calls=%all-reduce-scatter | all-reduce-scatter fusion | flops 131073 | bytes 459264
  175.4 8.2 %multiply_add_fusion.1 = f32[6,2,8,64,128]{4,3,2,1,0:T(8,128)} fusion(f32[6,2,8,64,128]{4,3,2,1,0:T(8,128)} %bitcast.210, f32[6,2,8]{2,1,0:T(2,128)S(1)} %negate_exponential_fusion.3, f32[6,4,2,8,64]{4,3,2,1,0:T(8,128)S(1)} %reshape.260, f32[6,4,2,8]{1,3,2,0:T(8,128)S(1)} %copy-done.12, f32[6,4,1,128,2]{3,1,4,0,2:T(4,128)S(1)} %copy-done.10), kind=kOutput, calls=%fused_computation.2 | convolution fusion | flops 39346176 | bytes 6416256 | tf_op jit(solution)/shard_map/sugrp,sugn->sgrpn/dot_general | solution.py:46
  187.9 32.9 %all-gather.1 = bf16[8,12,1024]{2,1,0:T(8,128)(2,1)} all-gather(bf16[1,12,1024]{2,1,0:T(8,128)(2,1)S(1)} %fusion.138), channel_id=1, replica_groups=mesh['tp'=8,'dp'=4] {'tp'}, dimensions={0}, use_global_device_ids=true | all-gather | bytes 221184 | tf_op jit(solution)/shard_map/all_gather | solution.py:52
  226.3 5.9 %all-reduce.8 = (f32[96,16]{0,1:T(8,128)S(1)}, f32[96]{0:T(128)S(1)}) all-reduce(f32[96,16]{0,1:T(8,128)S(1)} %fusion.30, f32[96]{0:T(128)S(1)} %get-tuple-element.34), channel_id=11, replica_groups=mesh['tp'=8,'dp'=4] {'dp'}, use_global_device_ids=true, to_apply=%region_12.13.clone | all-reduce | flops 1632 | bytes 13056
  233.3 2.9 fusion.6
  239.5 2.8 fusion.4
  245.5 31.3 %all_gather.22 = f32[6,4,2,2048]{3,1,2,0:T(4,128)S(1)} all-gather(f32[6,4,2,256]{3,1,2,0:T(4,128)S(1)} %divide_multiply_fusion.2), channel_id=1, replica_groups=mesh['tp'=8,'dp'=4] {'tp'}, dimensions={3}, use_global_device_ids=true | all-gather | bytes 442368 | tf_op jit(solution)/shard_map/all_gather | solution.py:124
  279.5 4.4 %constant_dynamic-slice_fusion = (f32[6,4,1,128,2]{4,3,1,2,0:T(8,128)}, f32[6,4,1,128,2]{4,3,1,2,0:T(8,128)}) fusion(f32[6,4,2,128,16]{4,3,1,2,0:T(8,128)} %reshape.308, s32[]{:T(128)S(6)} %select_n.55, s32[]{:T(128)S(6)} %add.254), kind=kLoop, calls=%fused_computation.215 | loop fusion | bytes 98312 | tf_op jit(solution)/shard_map/slice | solution.py:127
  288.8 8.1 %fusion.23 = f32[6,4,2,8,64]{4,1,3,2,0:T(4,128)} fusion(f32[6,2,8,64,128]{4,3,2,1,0:T(8,128)S(1)} %bitcast.207, f32[6,4,2,8]{1,3,2,0:T(8,128)S(1)} %copy-done.19, f32[6,4,1,128,2]{3,1,4,0,2:T(4,128)S(1)} %copy.144), kind=kOutput, calls=%fused_computation.28 | convolution fusion | flops 37773312 | bytes 3270144 | tf_op jit(solution)/shard_map/stgn,sgrpn->stgrp/dot_general | solution.py:41
  304.0 5.6 %all_gather.23 = bf16[96,1024]{1,0:T(8,128)(2,1)S(1)} all-gather(bf16[24,1024]{1,0:T(8,128)(2,1)S(1)} %fusion.80), channel_id=1, replica_groups=mesh['tp'=8,'dp'=4] {'dp'}, dimensions={0}, use_global_device_ids=true | all-gather | bytes 245760 | tf_op jit(solution)/shard_map/all_gather | solution.py:154
  309.6 2.8 fusion.2
  312.4 25.5 %fusion.1 = f32[16,1024]{1,0:T(8,128)S(1)} fusion(f32[96,1024]{1,0:T(8,128)} %fusion.2), kind=kCustom, calls=%all-reduce-scatter.1 | all-reduce-scatter fusion | flops 131073 | bytes 459264
  341.7 5.6 %multiply_add_fusion = f32[6,2,8,64,128]{4,3,2,1,0:T(8,128)S(1)} fusion(f32[6,2,8,64,128]{4,3,2,1,0:T(8,128)S(1)} %bitcast.208, f32[6,2,8]{2,1,0:T(2,128)S(1)} %negate_exponential_fusion.2, f32[6,4,2,8,64]{4,3,2,1,0:T(8,128)S(1)} %reshape.267, f32[6,4,2,8]{1,3,2,0:T(8,128)S(1)} %copy-done.11, f32[6,4,1,128,2]{3,1,4,0,2:T(4,128)S(1)} %copy-done.8), kind=kOutput, calls=%fused_computation.1 | convolution fusion | flops 39346176 | bytes 6416256 | tf_op jit(solution)/shard_map/sugrp,sugn->sgrpn/dot_general | solution.py:46
  347.3 3.3 pad_maximum_fusion
  (246 shorter events, 76.7 us)
Async XLA Ops:
  7.2 69.5 %reduce-scatter.15.cloned.1.call-start = ((), (), s32[]{:S(2)}) async-start(), calls=%async_computation.7 | async-start | bytes 245760 | tf_op jit(solution)/shard_map/reduce_scatter | solution.py:102
  45.5 86.8 %reduce-scatter.13.cloned.1.call-start = ((), (), s32[]{:S(2)}) async-start(), calls=%async_computation.6 | async-start | bytes 491520 | tf_op jit(solution)/shard_map/reduce_scatter | solution.py:101
  48.4 15.4 %copy-start.56 = (u32[32]{0:T(128)S(1)}, u32[32]{0:T(128)}, u32[]{:S(2)}) copy-start(u32[32]{0:T(128)} %constant.72) | copy-start | bytes 388
  48.4 17.3 %copy-start.43 = (bf16[2,4,2,256]{3,2,1,0:T(2,128)(2,1)S(1)}, bf16[2,4,2,256]{3,2,1,0:T(2,128)(2,1)}, u32[]{:S(2)}) copy-start(bf16[2,4,2,256]{3,2,1,0:T(2,128)(2,1)} %param.25) | copy-start | bytes 24580
  48.4 17.9 %copy-start.26 = (bf16[2,4,1024]{2,1,0:T(4,128)(2,1)S(1)}, bf16[2,4,1024]{2,1,0:T(4,128)(2,1)}, u32[]{:S(2)}) copy-start(bf16[2,4,1024]{2,1,0:T(4,128)(2,1)} %param.24) | copy-start | bytes 49156
  48.4 18.5 %copy-start.31 = (bf16[2,6,3,2,256]{4,3,2,1,0:T(2,128)(2,1)S(1)}, bf16[2,6,3,2,256]{4,3,2,1,0:T(2,128)(2,1)}, u32[]{:S(2)}) copy-start(bf16[2,6,3,2,256]{4,3,2,1,0:T(2,128)(2,1)} %param.29) | copy-start | bytes 110596
  48.5 19.2 %copy-start.6 = (bf16[2,6,3,1024]{3,0,2,1:T(2,128)(2,1)S(1)}, bf16[2,6,3,1024]{3,0,2,1:T(2,128)(2,1)}, u32[]{:S(2)}) copy-start(bf16[2,6,3,1024]{3,0,2,1:T(2,128)(2,1)} %param.28) | copy-start | bytes 221188
  48.5 88.1 %reduce-scatter.17.cloned.1.call-start = ((), (), s32[]{:S(2)}) async-start(), calls=%async_computation.8 | async-start | bytes 491520 | tf_op jit(solution)/shard_map/reduce_scatter | solution.py:100
  51.4 192.1 %reduce-scatter.21.cloned.1.call-start = ((), (), s32[]{:S(2)}) async-start(), calls=%async_computation.10 | async-start | bytes 245760 | tf_op jit(solution)/shard_map/reduce_scatter | solution.py:102
  116.6 14.8 %copy-start.22 = (bf16[6,4,2,256]{3,1,0,2:T(4,128)(2,1)S(1)}, bf16[6,4,2,256]{3,1,0,2:T(4,128)(2,1)}, u32[]{:S(2)}) copy-start(bf16[6,4,2,256]{3,1,0,2:T(4,128)(2,1)} %copy-done.21) | copy-start | bytes 73732
  116.6 14.8 %copy-start.25 = (bf16[1,6,3,2,256]{4,2,3,1,0:T(4,128)(2,1)S(1)}, bf16[1,6,3,2,256]{4,2,3,1,0:T(4,128)(2,1)}, u32[]{:S(2)}) copy-start(bf16[1,6,3,2,256]{4,2,3,1,0:T(4,128)(2,1)} %copy-done.24) | copy-start | bytes 55300
  116.6 14.8 %copy-start.50 = (s32[6,3]{1,0:T(8,128)S(1)}, s32[6,3]{1,0:T(8,128)}, u32[]{:S(2)}) copy-start(s32[6,3]{1,0:T(8,128)} %iota_add_fusion) | copy-start | bytes 220
  116.6 15.6 %copy-start.42 = (f32[24]{0:T(128)S(1)}, f32[24]{0:T(128)}, u32[]{:S(2)}) copy-start(f32[24]{0:T(128)} %copy-done.41) | copy-start | bytes 292
  136.6 38.9 %copy-start.10 = (f32[6,4,1,128,2]{3,1,4,0,2:T(4,128)S(1)}, f32[6,4,1,128,2]{3,1,4,0,2:T(4,128)}, u32[]{:S(2)}) copy-start(f32[6,4,1,128,2]{3,1,4,0,2:T(4,128)} %copy-done.9) | copy-start | bytes 73732
  136.6 38.9 %copy-start.12 = (f32[6,4,2,8]{1,3,2,0:T(8,128)S(1)}, f32[6,4,2,8]{1,3,2,0:T(8,128)}, u32[]{:S(2)}) copy-start(f32[6,4,2,8]{1,3,2,0:T(8,128)} %copy.114) | copy-start | bytes 4612
  171.9 13.2 %collective-permute-start = (f32[16,1024]{1,0:T(8,128)S(1)}, f32[16,1024]{1,0:T(8,128)}, u32[]{:S(2)}, u32[]{:S(2)}) collective-permute-start(f32[16,1024]{1,0:T(8,128)S(1)} %fusion), channel_id=1, source_target_pairs={{0,4},{4,8},{8,12},{12,16},{16,20},{20,24},{24,28},{1,5},{5,9},{9,... | collective-permute-start | bytes 196616
  173.9 10.6 %collective-permute-start.1 = (f32[12,1024]{1,0:T(8,128)S(1)}, f32[12,1024]{1,0:T(8,128)S(1)}, u32[]{:S(2)}, u32[]{:S(2)}) collective-permute-start(f32[12,1024]{1,0:T(8,128)S(1)} %slice.288), channel_id=1, source_target_pairs={{0,8},{4,12},{8,16},{12,20},{16,24},{20,28},{1,9},{5,13},{9,17},{1... | collective-permute-start | bytes 147464
  183.6 48.9 %copy-start.49 = (f32[2,8]{1,0:T(2,128)S(1)}, f32[2,8]{1,0:T(2,128)}, u32[]{:S(2)}) copy-start(f32[2,8]{1,0:T(2,128)} %add.222) | copy-start | bytes 196
  226.2 70.7 %reduce-scatter.19.cloned.1.call-start = ((), (), s32[]{:S(2)}) async-start(), calls=%async_computation.9 | async-start | bytes 491520 | tf_op jit(solution)/shard_map/reduce_scatter | solution.py:101
  236.3 66.7 %reduce-scatter.23.cloned.1.call-start = ((), (), s32[]{:S(2)}) async-start(), calls=%async_computation.11 | async-start | bytes 491520 | tf_op jit(solution)/shard_map/reduce_scatter | solution.py:100
  301.2 40.4 %copy-start.8 = (f32[6,4,1,128,2]{3,1,4,0,2:T(4,128)S(1)}, f32[6,4,1,128,2]{3,1,4,0,2:T(4,128)}, u32[]{:S(2)}) copy-start(f32[6,4,1,128,2]{3,1,4,0,2:T(4,128)} %copy-done.7) | copy-start | bytes 73732
  301.2 40.4 %copy-start.11 = (f32[6,4,2,8]{1,3,2,0:T(8,128)S(1)}, f32[6,4,2,8]{1,3,2,0:T(8,128)}, u32[]{:S(2)}) copy-start(f32[6,4,2,8]{1,3,2,0:T(8,128)} %copy.116) | copy-start | bytes 4612
  337.9 14.1 %collective-permute-start.2 = (f32[16,1024]{1,0:T(8,128)S(1)}, f32[16,1024]{1,0:T(8,128)}, u32[]{:S(2)}, u32[]{:S(2)}) collective-permute-start(f32[16,1024]{1,0:T(8,128)S(1)} %fusion.1), channel_id=1, source_target_pairs={{0,4},{4,8},{8,12},{12,16},{16,20},{20,24},{24,28},{1,5},{5,9},{9,... | collective-permute-start | bytes 196616
  340.1 11.3 %collective-permute-start.3 = (f32[12,1024]{1,0:T(8,128)S(1)}, f32[12,1024]{1,0:T(8,128)S(1)}, u32[]{:S(2)}, u32[]{:S(2)}) collective-permute-start(f32[12,1024]{1,0:T(8,128)S(1)} %slice.289), channel_id=1, source_target_pairs={{0,8},{4,12},{8,16},{12,20},{16,24},{20,28},{1,9},{5,13},{9,17},{1... | collective-permute-start | bytes 147464
  (44 other events, 417.1 us)
Sparse Core Ops, SparseCore 0:
  45.5 20.7 reduce-scatter.14
  68.9 20.8 reduce-scatter.12
  92.2 20.8 reduce-scatter.16
  226.4 17.1 reduce-scatter.20
  245.9 20.7 reduce-scatter.18
  269.1 20.7 reduce-scatter.22
where the time goes:
time: 368 us; the launch traced here: 363 us
  blocking collectives  202 us (55%)
  matrix products  61.6 us (17%)
  local copies, waits for them, and re-layouts  56.8 us (15%)
  between operations  16.7 us (5%)
  other arithmetic  16.3 us (4%)
  starting transfers between devices  7.53 us (2%)
    all_gather x2, blocking collectives, collect(): return lax.all_gather(token_rows, 'tp', axis=0, tiled=True)  65.6 us
    unnamed x4, blocking collectives  62.9 us
    all_gather x2, blocking collectives, body(): vector_whole = lax.all_gather(vector_conv, 'tp', axis=3, tiled=True)  62.4 us
    unnamed x132, local copies, waits for them, and re-layouts  19.1 us
    dot_general x2, matrix products, state_block(): jnp.einsum('stgn,sgrpn->stgrp', read_vec, carried_state, precision=highest)  18 us
    dot_general x2, matrix products, state_block(): jnp.einsum('sugrp,sugn->sgrpn', weighted, write_vec, precision=highest)  13.8 us
    all_gather x2, blocking collectives, body(): mixed_all = lax.all_gather(mixed, 'dp', axis=0, tiled=True)  11.4 us
    slice x2, local copies, waits for them, and re-layouts, body(): write_vec = jnp.swapaxes(own_vectors[:, :, 0], 2, 3)  8.8 us
  transfers between devices with their start and end apart: 10, of which 1 were waited for; matrix products, arithmetic and copies ran while one was open for 30% of the time, Pallas kernels for 0%

commit v1 on v0

--- a/solution.py
+++ b/solution.py
@@ -1,6 +1,10 @@
+import functools
+
 import jax
 import jax.numpy as jnp
 from jax import lax
+from jax.experimental import pallas as pl
+from jax.experimental.pallas import tpu as pltpu
 from jax.sharding import PartitionSpec as P
 
 D = 4096
@@ -165,9 +169,425 @@
     return (token_rows, jnp.stack(state_list), jnp.stack(value_list), jnp.stack(vector_list))
 
 
+BF = jnp.bfloat16
+F32 = jnp.float32
+SUB = 8
+
+
+def one_hot(cond):
+    return jnp.where(cond, 1.0, 0.0).astype(BF)
+
+
+def grid_of(shape, dim):
+    return lax.broadcasted_iota(jnp.int32, shape, dim)
+
+
+def dot(a, b):
+    return jnp.dot(a, b, preferred_element_type=F32)
+
+
+def dot_nt(a, b):
+    return lax.dot_general(a, b, (((1,), (1,)), ((), ())), preferred_element_type=F32)
+
+
+def silu(x):
+    return x * (1.0 / (1.0 + jnp.exp(-x)))
+
+
+def softplus(x):
+    return jnp.maximum(x, 0.0) + jnp.log1p(jnp.exp(-jnp.abs(x)))
+
+
+def conv_rows(old, fresh, taps):
+    padded = [old[SUB * k : SUB * (k + 1)] for k in range(CONV - 1)]
+    padded = padded + [fresh[SUB * t : SUB * (t + 1)] for t in range(NEW)]
+    outs = []
+    for t in range(NEW):
+        total = padded[t] * taps[0:1]
+        for k in range(1, CONV):
+            total = total + padded[t + k] * taps[k : k + 1]
+        outs.append(silu(total))
+    return outs, padded
+
+
+def keep_rows(padded, lens):
+    rows = []
+    for j in range(CONV - 1):
+        row = padded[j]
+        for length in range(1, NEW + 1):
+            row = jnp.where(lens == length, padded[length + j], row)
+        rows.append(row)
+    return jnp.concatenate(rows, axis=0)
+
+
+def step_kernel(
+    n_tp, n_dp, sizes,
+    tok_ref, lens_ref, gain_ref, bias_ref, rate_ref, vtap_ref, ctap_ref, vhist_ref, chist_ref,
+    gw_hbm, vw_hbm, cw_hbm, sw_hbm, ow_hbm, st_hbm,
+    out_ref, nvh_ref, nch_ref, zt_ref, wr_ref,
+    gw, vw, cw, sw, ow, st, whole, x32, tok, send_c, recv_c, send_v, recv_v, send_g, recv_g,
+    send_w, recv_w, send_m, recv_m, acc, send_o, recv_o,
+    load_sem, own_sem, ag_s, ag_r, rs_s, rs_r, vx_s, vx_r, mx_s, mx_r, ox_s, ox_r,
+):
+    rows, seqs = sizes
+    block = seqs * NEW
+    chans = vw.shape[2]
+    vcols = cw.shape[2] // 2
+    me_tp, me_dp = lax.axis_index("tp"), lax.axis_index("dp")
+    barrier = pltpu.get_barrier_semaphore()
+    for k in range(1, n_tp):
+        pl.semaphore_signal(
+            barrier, inc=1, device_id={"tp": lax.rem(me_tp + k, n_tp)},
+            device_id_type=pl.DeviceIdType.MESH,
+        )
+    for k in range(1, n_dp):
+        pl.semaphore_signal(
+            barrier, inc=1, device_id={"dp": lax.rem(me_dp + k, n_dp)},
+            device_id_type=pl.DeviceIdType.MESH,
+        )
+    loads = {}
+    for layer in range(LAYERS):
+        for slot, (name, src, dst) in enumerate(
+            (("c", cw_hbm, cw), ("s", sw_hbm, sw), ("v", vw_hbm, vw), ("g", gw_hbm, gw),
+             ("st", st_hbm, st), ("o", ow_hbm, ow))
+        ):
+            copy = pltpu.make_async_copy(src.at[layer], dst.at[layer], load_sem.at[layer, slot])
+            copy.start()
+            loads[layer, name] = copy
+    pl.semaphore_wait(barrier, n_tp + n_dp - 2)
+    pending = []
+
+    def exchange(axis, n, me, source, target, s_sem, r_sem):
+        waits = []
+        for k in range(1, n):
+            peer = lax.rem(me + k, n)
+            copy = pltpu.make_async_remote_copy(
+                src_ref=source(peer), dst_ref=target.at[me], send_sem=s_sem.at[k],
+                recv_sem=r_sem.at[k], device_id={axis: peer},
+                device_id_type=pl.DeviceIdType.MESH,
+            )
+            copy.start()
+            pending.append(copy)
+            origin = lax.rem(me + n - k, n)
+            waits.append(
+                pltpu.make_async_remote_copy(
+                    src_ref=target.at[origin], dst_ref=target.at[origin], send_sem=s_sem.at[k],
+                    recv_sem=r_sem.at[k], device_id={axis: peer},
+                    device_id_type=pl.DeviceIdType.MESH,
+                )
+            )
+        return waits
+
+    lens = lens_ref[:, 0:1]
+    live = [jnp.where(lens > t, 1.0, 0.0) for t in range(NEW)]
+    big = NEW * SUB
+    pr, pc = grid_of((big, block), 0), grid_of((big, block), 1)
+    spread = one_hot(((pr & (SUB - 1)) < seqs) & (pc == (pr & (SUB - 1)) * NEW + (pr >> 3)))
+    qr, qc = grid_of((block, big), 0), grid_of((block, big), 1)
+    gather = one_hot((qr >> 2) + (qr & (NEW - 1)) * SUB == qc)
+    heads_all = sw.shape[2]
+    er, ec = grid_of((heads_all, chans), 0), grid_of((heads_all, chans), 1)
+    expand = one_hot(er == me_tp * (chans // HEAD_DIM) + ec // HEAD_DIM)
+    orow, ocol = grid_of((vcols, vcols), 0), grid_of((vcols, vcols), 1)
+    part_n = vcols // GROUPS
+    perm = one_hot(ocol == (orow & (part_n - 1)) * GROUPS + orow // part_n)
+    groups = GROUPS // n_tp
+    per = chans // groups
+    seq_of_row = grid_of((big, STATE), 0) & (SUB - 1)
+
+    for layer in range(LAYERS):
+        mine = tok_ref if layer == 0 else tok
+        wide = whole.at[layer]
+        waits = exchange("tp", n_tp, me_tp, lambda peer: mine, wide, ag_s.at[layer], ag_r.at[layer])
+        own = pltpu.make_async_copy(mine, wide.at[me_tp], own_sem.at[layer])
+        own.start()
+        own.wait()
+        for w in waits:
+            w.wait_recv()
+        for i in range(n_tp):
+            x32[rows * i : rows * (i + 1), :] = wide[i].astype(F32)
+        x = x32[...]
+        squares = jnp.sum(x * x, axis=1, keepdims=True)
+        normed = (x * gain_ref[layer : layer + 1]).astype(BF)
+
+        def scatter(parts, send, recv, which):
+            at = 0
+            for part in parts:
+                width = part.shape[1]
+                for d in range(n_dp):
+                    send[layer, d, :, at : at + width] = part[block * d : block * (d + 1)].astype(BF)
+                at = at + width
+            return exchange(
+                "dp", n_dp, me_dp, lambda peer: send.at[layer, peer], recv.at[layer],
+                rs_s.at[layer, which], rs_r.at[layer, which],
+            )
+
+        def settle(waits, send, recv):
+            total = send[layer, me_dp].astype(F32)
+            for k, w in enumerate(waits):
+                w.wait_recv()
+                total = total + recv[layer, lax.rem(me_dp + n_dp - 1 - k, n_dp)].astype(F32)
+            return total
+
+        loads[layer, "c"].wait()
+        vec_part = dot(normed, cw[layer])
+        loads[layer, "s"].wait()
+        step_part = dot(normed, sw[layer])
+        lane = grid_of((rows * n_tp, 128), 1)
+        high = squares.astype(BF).astype(F32)
+        sq_part = jnp.where(lane == 0, high, jnp.where(lane == 1, squares - high, 0.0))
+        waits_c = scatter((vec_part, step_part, sq_part), send_c, recv_c, 0)
+        loads[layer, "v"].wait()
+        waits_v = scatter((dot(normed, vw[layer]),), send_v, recv_v, 1)
+        loads[layer, "g"].wait()
+        waits_g = scatter((dot(normed, gw[layer]),), send_g, recv_g, 2)
+
+        sums = settle(waits_c, send_c, recv_c)
+        vwide = 2 * vcols
+        total_sq = jnp.sum(sums[:, vwide + heads_all :], axis=1, keepdims=True)
+        scaling = lax.rsqrt(total_sq / D + norm_floor)
+        small = dot(spread, (sums[:, : vwide + heads_all] * scaling).astype(BF))
+        conv, padded = conv_rows(
+            chist_ref[layer].astype(F32), small[:, :vwide], ctap_ref[layer]
+        )
+        nch_ref[layer] = keep_rows(padded, lens).astype(BF)
+        conv = jnp.concatenate(conv, axis=0)
+        stacked = jnp.concatenate(
+            [conv[:, :vcols], conv[:, vcols:], jnp.zeros((128 - 2 * big, vcols), F32)], axis=0
+        ).astype(BF)
+        turned = dot_nt(perm, stacked).astype(BF)
+        each = vcols // n_tp
+        for j in range(n_tp):
+            send_w[layer, j] = turned[each * j : each * (j + 1)]
+        waits_w = exchange(
+            "tp", n_tp, me_tp, lambda peer: send_w.at[layer, peer], recv_w.at[layer],
+            vx_s.at[layer], vx_r.at[layer],
+        )
+        recv_w[layer, me_tp] = send_w[layer, me_tp]
+
+        steps_wide = dot(expand_rows(small, vwide), expand) + bias_ref[layer : layer + 1]
+        steps_wide = softplus(steps_wide)
+        step = [steps_wide[SUB * t : SUB * (t + 1)] * live[t] for t in range(NEW)]
+        rate = rate_ref[layer : layer + 1]
+        cum = [step[0] * rate]
+        for t in range(1, NEW):
+            cum.append(cum[-1] + step[t] * rate)
+        values_in = dot(spread, (settle(waits_v, send_v, recv_v) * scaling).astype(BF))
+        value, padded = conv_rows(vhist_ref[layer].astype(F32), values_in, vtap_ref[layer])
+        nvh_ref[layer] = keep_rows(padded, lens).astype(BF)
+        stepped = [step[t] * value[t] for t in range(NEW)]
+        ending = [jnp.exp(cum[t] - cum[NEW - 1]) * stepped[t] for t in range(NEW)]
+        gate_in = dot(spread, (settle(waits_g, send_g, recv_g) * scaling).astype(BF))
+        gates = silu(gate_in)
+        zrows = jnp.concatenate(
+            ending + [jnp.exp(-cum[NEW - 1]), jnp.zeros((128 - big - SUB, chans), F32)], axis=0
+        )
+        zt_ref[layer] = zrows.T
+
+        for w in waits_w:
+            w.wait_recv()
+        loads[layer, "st"].wait()
+        half = each // groups
+        y_parts = [[] for _ in range(NEW)]
+        for g in range(groups):
+            tall = jnp.concatenate(
+                [recv_w[layer, i, half * g : half * (g + 1), :].astype(F32) for i in range(n_tp)],
+                axis=0,
+            )
+            flat = tall.T
+            write, read = flat[:big], flat[big : 2 * big]
+            wr_ref[layer, g] = write.astype(BF)
+            carried = jnp.zeros((big, per), F32)
+            for s in range(seqs):
+                picked = jnp.where(seq_of_row == s, read, 0.0).astype(BF)
+                carried = carried + dot_nt(
+                    picked, st[layer, s, per * g : per * (g + 1), :].astype(BF)
+                )
+            span = slice(per * g, per * (g + 1))
+            for t in range(NEW):
+                now = cum[t][:, span]
+                y = carried[SUB * t : SUB * (t + 1)] * jnp.exp(-now)
+                for u in range(t + 1):
+                    score = jnp.sum(
+                        read[SUB * t : SUB * (t + 1)] * write[SUB * u : SUB * (u + 1)],
+                        axis=1, keepdims=True,
+                    )
+                    y = y + score * jnp.exp(cum[u][:, span] - now) * stepped[u][:, span]
+                y_parts[t].append(y)
+        mixed = jnp.concatenate(
+            [
+                jnp.concatenate(y_parts[t], axis=1) * gates[SUB * t : SUB * (t + 1)] * live[t]
+                for t in range(NEW)
+            ],
+            axis=0,
+        ).astype(BF)
+        send_m[layer] = dot(gather, mixed).astype(BF)
+        waits = exchange(
+            "dp", n_dp, me_dp, lambda peer: send_m.at[layer], recv_m.at[layer],
+            mx_s.at[layer], mx_r.at[layer],
+        )
+        recv_m[layer, me_dp] = send_m[layer]
+        for w in waits:
+            w.wait_recv()
+        loads[layer, "o"].wait()
+        mixed_all = jnp.concatenate([recv_m[layer, d] for d in range(n_dp)], axis=0)
+        acc[...] = dot(mixed_all, ow[layer])
+        for j in range(n_tp):
+            send_o[layer, j] = acc[rows * j : rows * (j + 1), :].astype(BF)
+        waits = exchange(
+            "tp", n_tp, me_tp, lambda peer: send_o.at[layer, peer], recv_o.at[layer],
+            ox_s.at[layer], ox_r.at[layer],
+        )
+        total = send_o[layer, me_tp].astype(F32)
+        for k, w in enumerate(waits):
+            w.wait_recv()
+            total = total + recv_o[layer, lax.rem(me_tp + n_tp - 1 - k, n_tp)].astype(F32)
+        fresh = (mine[...].astype(F32) + total).astype(BF)
+        if layer + 1 < LAYERS:
+            tok[...] = fresh
+        else:
+            out_ref[...] = fresh
+    for copy in pending:
+        copy.wait_send()
+
+
+def expand_rows(small, start):
+    return small[:, start:].astype(BF)
+
+
+def state_kernel(seqs, zt_ref, wr_ref, st_ref, out_ref):
+    zt = zt_ref[0]
+    big = NEW * SUB
+    weighted = zt[:, :big].astype(BF)
+    write = wr_ref[0, 0].astype(F32)
+    seq_of_row = grid_of((big, STATE), 0) & (SUB - 1)
+    for s in range(seqs):
+        picked = jnp.where(seq_of_row == s, write, 0.0).astype(BF)
+        out_ref[0, s] = zt[:, big + s : big + s + 1] * st_ref[0, s] + dot(weighted, picked)
+
+
+def fast_body(
+    n_tp, n_dp,
+    tokens, lengths, norm_gain, gate_weight, value_weight, vector_weight, step_weight, step_bias,
+    decay_rate, value_taps, vector_taps, out_weight, recurrent_state, value_history, vector_history,
+):
+    rows, feats = tokens.shape
+    seqs = lengths.shape[0]
+    block = seqs * NEW
+    chans = value_weight.shape[2]
+    vwide = 2 * vector_weight.shape[3]
+    heads_all = step_weight.shape[2]
+    lens = jnp.broadcast_to(jnp.pad(lengths, (0, SUB - seqs))[:, None], (SUB, 128))
+    wide_bias = jnp.repeat(step_bias, HEAD_DIM, axis=1)
+    wide_rate = jnp.repeat(decay_rate, HEAD_DIM, axis=1)
+    pad = ((0, 0), (0, 0), (0, SUB - seqs), (0, 0))
+    vhist = jnp.pad(jnp.swapaxes(value_history, 1, 2), pad).reshape(LAYERS, -1, chans)
+    chist = vector_history.reshape(LAYERS, seqs, CONV - 1, vwide)
+    chist = jnp.pad(jnp.swapaxes(chist, 1, 2), pad).reshape(LAYERS, -1, vwide)
+    state = recurrent_state.reshape(LAYERS, seqs, chans, STATE)
+    groups = GROUPS // n_tp
+    big = NEW * SUB
+    csum = vwide + heads_all + 128
+    vm, hb = pl.BlockSpec(memory_space=pltpu.VMEM), pl.BlockSpec(memory_space=pl.ANY)
+    dma = pltpu.SemaphoreType.DMA
+    each = vwide // 2 // n_tp
+    fresh, nvh, nch, zt, wr = pl.pallas_call(
+        functools.partial(step_kernel, n_tp, n_dp, (rows, seqs)),
+        out_shape=(
+            jax.ShapeDtypeStruct((rows, feats), BF),
+            jax.ShapeDtypeStruct((LAYERS, (CONV - 1) * SUB, chans), BF),
+            jax.ShapeDtypeStruct((LAYERS, (CONV - 1) * SUB, vwide), BF),
+            jax.ShapeDtypeStruct((LAYERS, chans, 128), F32),
+            jax.ShapeDtypeStruct((LAYERS, groups, big, STATE), BF),
+        ),
+        in_specs=[vm] * 9 + [hb] * 6,
+        out_specs=(vm,) * 5,
+        scratch_shapes=[
+            pltpu.VMEM((LAYERS, feats, chans), BF),
+            pltpu.VMEM((LAYERS, feats, chans), BF),
+            pltpu.VMEM((LAYERS, feats, vwide), BF),
+            pltpu.VMEM((LAYERS, feats, heads_all), BF),
+            pltpu.VMEM((LAYERS, chans, feats), BF),
+            pltpu.VMEM((LAYERS, seqs, chans, STATE), F32),
+            pltpu.VMEM((LAYERS, n_tp, rows, feats), BF),
+            pltpu.VMEM((n_tp * rows, feats), F32),
+            pltpu.VMEM((rows, feats), BF),
+            pltpu.VMEM((LAYERS, n_dp, block, csum), BF),
+            pltpu.VMEM((LAYERS, n_dp, block, csum), BF),
+            pltpu.VMEM((LAYERS, n_dp, block, chans), BF),
+            pltpu.VMEM((LAYERS, n_dp, block, chans), BF),
+            pltpu.VMEM((LAYERS, n_dp, block, chans), BF),
+            pltpu.VMEM((LAYERS, n_dp, block, chans), BF),
+            pltpu.VMEM((LAYERS, n_tp, each, 128), BF),
+            pltpu.VMEM((LAYERS, n_tp, each, 128), BF),
+            pltpu.VMEM((LAYERS, block, chans), BF),
+            pltpu.VMEM((LAYERS, n_dp, block, chans), BF),
+            pltpu.VMEM((n_tp * rows, feats), F32),
+            pltpu.VMEM((LAYERS, n_tp, rows, feats), BF),
+            pltpu.VMEM((LAYERS, n_tp, rows, feats), BF),
+            dma((LAYERS, 6)),
+            dma((LAYERS,)),
+            dma((LAYERS, n_tp)), dma((LAYERS, n_tp)),
+            dma((LAYERS, 3, n_dp)), dma((LAYERS, 3, n_dp)),
+            dma((LAYERS, n_tp)), dma((LAYERS, n_tp)),
+            dma((LAYERS, n_dp)), dma((LAYERS, n_dp)),
+            dma((LAYERS, n_tp)), dma((LAYERS, n_tp)),
+        ],
+        compiler_params=pltpu.CompilerParams(
+            collective_id=0, has_side_effects=True, vmem_limit_bytes=56 * 1024 * 1024
+        ),
+        name="step_kernel",
+    )(
+        tokens, lens, norm_gain, wide_bias, wide_rate, value_taps.astype(F32),
+        vector_taps.reshape(LAYERS, CONV, vwide).astype(F32), vhist, chist,
+        gate_weight, value_weight, vector_weight.reshape(LAYERS, feats, vwide), step_weight,
+        out_weight, state,
+    )
+    cut = chans // groups // 2
+    next_state = pl.pallas_call(
+        functools.partial(state_kernel, seqs),
+        grid=(LAYERS, chans // cut),
+        out_shape=jax.ShapeDtypeStruct(state.shape, F32),
+        in_specs=[
+            pl.BlockSpec((1, cut, 128), lambda l, c: (l, c, 0)),
+            pl.BlockSpec((1, 1, big, STATE), lambda l, c: (l, c // 2, 0, 0)),
+            pl.BlockSpec((1, seqs, cut, STATE), lambda l, c: (l, 0, c, 0)),
+        ],
+        out_specs=pl.BlockSpec((1, seqs, cut, STATE), lambda l, c: (l, 0, c, 0)),
+        name="state_kernel",
+    )(zt, wr, state)
+
+    def unpack(rows_of, width):
+        return jnp.swapaxes(rows_of.reshape(LAYERS, CONV - 1, SUB, width)[:, :, :seqs], 1, 2)
+
+    return (
+        fresh,
+        next_state.reshape(recurrent_state.shape),
+        unpack(nvh, chans),
+        unpack(nch, vwide).reshape(vector_history.shape),
+    )
+
+
+def choose(n_tp, n_dp, *args):
+    tokens, lengths = args[0], args[1]
+    fits = (
+        GROUPS % n_tp == 0
+        and args[7].shape[1] * n_tp == HEADS
+        and args[5].shape[3] % 128 == 0
+        and tokens.shape[1] % 128 == 0
+        and tokens.shape[0] % 4 == 0
+        and lengths.shape[0] <= SUB
+        and args[5].shape[3] // GROUPS >= 16
+        and tokens.shape[0] * n_tp == lengths.shape[0] * NEW * n_dp
+    )
+    if fits:
+        return fast_body(n_tp, n_dp, *args)
+    return body(*args)
+
+
 def solution(mesh):
     return jax.shard_map(
-        body,
+        functools.partial(choose, mesh.shape['tp'], mesh.shape['dp']),
         mesh=mesh,
         in_specs=(
             P("tp", "dp"),

time: 368 us -> 93.7 us (0.25); the launches traced: 363 us -> 93 us
  blocking collectives: 202 us -> 0 us
  Pallas kernels: 0 us -> 74.4 us
  matrix products: 61.6 us -> 0 us
  local copies, waits for them, and re-layouts: 56.8 us -> 16.6 us
  between operations: 16.7 us -> 0.68 us
  other arithmetic: 16.3 us -> 1.33 us
  starting transfers between devices: 7.53 us -> 0 us
    all_gather x6 -> x0, blocking collectives: 139 us -> none  [the longest x2 65.6 us: collect(): return lax.all_gather(token_rows, 'tp', axis=0, tiled=True)]
    pallas_call x0 -> x2, Pallas kernels: none -> 74.4 us  [the longest x1 65.3 us: fast_body(): pl.pallas_call(functools.partial(step_kernel, n_tp, n_dp, (rows, seqs)),...]
    unnamed x4 -> x0, blocking collectives: 62.9 us -> none
    dot_general x22 -> x0, matrix products: 61.6 us -> none  [the longest x2 18 us: state_block(): jnp.einsum('stgn,sgrpn->stgrp', read_vec, carried_state, precision=highest)]
    slice x9 -> x0, local copies, waits for them, and re-layouts: 19.3 us -> none  [the longest x2 8.8 us: body(): write_vec = jnp.swapaxes(own_vectors[:, :, 0], 2, 3)]
    unnamed x132 -> x9, local copies, waits for them, and re-layouts: 19.1 us -> 5.4 us
    unnamed x4 -> x0, starting transfers between devices: 7.28 us -> none
    convert_element_type x8 -> x1, other arithmetic: 7.4 us -> 1.33 us  [fast_body(): value_taps.astype(F32)]
  transfers between devices with their start and end apart: 10 -> 0, of which waited for: 1 -> 0; matrix products, arithmetic and copies ran while one was open for 30% -> 0% of each run, Pallas kernels for 0% -> 0%
where the time goes in v1:
time: 93.7 us; the launch traced here: 93 us
  Pallas kernels  74.4 us (79%)
  local copies, waits for them, and re-layouts  16.6 us (18%)
  other arithmetic  1.33 us (1%)
    pallas_call x1, Pallas kernels, fast_body(): pl.pallas_call(functools.partial(step_kernel, n_tp, n_dp, (rows, seqs)),...  65.3 us
    pallas_call x1, Pallas kernels, fast_body(): pl.pallas_call(functools.partial(state_kernel, seqs), grid=(LAYERS, chans...  9.1 us
    unnamed x9, local copies, waits for them, and re-layouts  5.4 us
    reshape x1, local copies, waits for them, and re-layouts, fast_body(): vector_weight.reshape(LAYERS, feats, vwide)  4.37 us

profile of v1, /device:TPU:0, one launch (start us, length us, event | category | flops | bytes accessed | tf_op | source)
XLA Modules:
  0.0 93.0 jit_solution(16769325792404907388)
XLA Ops:
  0.6 0.7 pad.12
  1.3 0.7 broadcast_in_dim.12.lens_ref
  2.0 0.7 broadcast_in_dim.13
  2.7 0.7 reshape.45.bias_ref
  3.4 0.7 broadcast_in_dim.14
  4.1 0.7 reshape.46.rate_ref
  4.8 1.3 %reshape.56.ctap_ref = f32[2,4,512]{2,1,0:T(4,128)} reshape(bf16[2,4,2,256]{3,2,1,0:T(2,128)(2,1)} %param.25) | data formatting | bytes 24576 | tf_op jit(solution)/shard_map/convert_element_type | solution.py:542
  6.1 1.3 %convert_element_type.12.vtap_ref = f32[2,4,1024]{2,1,0:T(4,128)} convert(bf16[2,4,1024]{2,1,0:T(4,128)(2,1)} %param.24) | non-fusion elementwise | flops 8192 | bytes 49152 | tf_op jit(solution)/shard_map/convert_element_type | solution.py:541
  7.5 0.8 copy.24
  8.3 0.6 pad_bitcast_fusion.1.chist_ref
  8.9 0.9 copy.31
  9.8 0.6 pad_bitcast_fusion.vhist_ref
  10.5 4.4 %reshape.50.cw_hbm = bf16[2,1024,512]{2,1,0:T(8,128)(2,1)} reshape(bf16[2,1024,2,256]{3,2,1,0:T(2,128)(2,1)} %param.20) | data formatting | bytes 4194304 | tf_op jit(solution)/shard_map/reshape | solution.py:543
  14.9 65.3 %step_kernel.1 = (bf16[12,1024]{1,0:T(8,128)(2,1)}, bf16[2,24,1024]{2,1,0:T(8,128)(2,1)}, bf16[2,24,512]{2,1,0:T(8,128)(2,1)}, f32[2,1024,128]{2,1,0:T(8,128)}, bf16[2,2,32,128]{3,2,1,0:T(8,128)(2,1)}) custom-call(bf16[12,1024]{1,0:T(8,128)(2,1)} %tok_ref.1, s32[8,128]{1,0:T(8,128)} %broadcast_in_dim.12.lens_ref, f32[2,1024]{1,0:T(2,128)} %gain_ref.1, ...), custom_call_target="tpu_custom_call" | custom-call | tf_op jit(solution)/shard_map/step_kernel/pallas_call | solution.py:494
  80.1 0.8 copy.36
  81.0 0.6 copy.28
  81.6 1.6 %copy.35 = bf16[2,3,6,1024]{3,0,1,2:T(2,128)(2,1)} copy(bf16[2,3,6,1024]{3,2,1,0:T(8,128)(2,1)} %bitcast.27) | data formatting | bytes 147456
  83.2 0.0 copy-start
  83.2 9.1 %state_kernel.1 = f32[2,6,1024,128]{3,2,1,0:T(8,128)} custom-call(f32[2,1024,128]{2,1,0:T(8,128)} %get-tuple-element.10.zt_ref, bf16[2,2,32,128]{3,2,1,0:T(8,128)(2,1)} %get-tuple-element.11.wr_ref, f32[2,6,1024,128]{3,2,1,0:T(8,128)} %bitcast.23), custom_call_target="tpu_custom_call" | custom-call | tf_op jit(solution)/shard_map/state_kernel/pallas_call | solution.py:547
  92.3 0.0 copy-done
  92.3 0.6 copy.38
  (3 shorter events, 0.1 us)
Async XLA Ops:
  83.2 9.1 %copy-start = (bf16[12,1024]{1,0:T(8,128)(2,1)S(1)}, bf16[12,1024]{1,0:T(8,128)(2,1)}, u32[]{:S(2)}) copy-start(bf16[12,1024]{1,0:T(8,128)(2,1)} %get-tuple-element.22) | copy-start | bytes 73732

commit v2 on v1

--- a/solution.py
+++ b/solution.py
@@ -203,9 +203,9 @@
     padded = padded + [fresh[SUB * t : SUB * (t + 1)] for t in range(NEW)]
     outs = []
     for t in range(NEW):
-        total = padded[t] * taps[0:1]
+        total = padded[t] * taps[0]
         for k in range(1, CONV):
-            total = total + padded[t + k] * taps[k : k + 1]
+            total = total + padded[t + k] * taps[k]
         outs.append(silu(total))
     return outs, padded
 
@@ -225,7 +225,7 @@
     tok_ref, lens_ref, gain_ref, bias_ref, rate_ref, vtap_ref, ctap_ref, vhist_ref, chist_ref,
     gw_hbm, vw_hbm, cw_hbm, sw_hbm, ow_hbm, st_hbm,
     out_ref, nvh_ref, nch_ref, zt_ref, wr_ref,
-    gw, vw, cw, sw, ow, st, whole, x32, tok, send_c, recv_c, send_v, recv_v, send_g, recv_g,
+    gw, vw, cw, raw, vhs, chs, sw, ow, st, whole, x32, tok, send_c, recv_c, send_v, recv_v, send_g, recv_g,
     send_w, recv_w, send_m, recv_m, acc, send_o, recv_o,
     load_sem, own_sem, ag_s, ag_r, rs_s, rs_r, vx_s, vx_r, mx_s, mx_r, ox_s, ox_r,
 ):
@@ -248,7 +248,7 @@
     loads = {}
     for layer in range(LAYERS):
         for slot, (name, src, dst) in enumerate(
-            (("c", cw_hbm, cw), ("s", sw_hbm, sw), ("v", vw_hbm, vw), ("g", gw_hbm, gw),
+            (("c", cw_hbm, raw), ("s", sw_hbm, sw), ("v", vw_hbm, vw), ("g", gw_hbm, gw),
              ("st", st_hbm, st), ("o", ow_hbm, ow))
         ):
             copy = pltpu.make_async_copy(src.at[layer], dst.at[layer], load_sem.at[layer, slot])
@@ -278,7 +278,11 @@
             )
         return waits
 
-    lens = lens_ref[:, 0:1]
+    who = grid_of((SUB, 128), 0)
+    lens = jnp.zeros((SUB, 128), jnp.int32)
+    for s in range(seqs):
+        lens = jnp.where(who == s, lens_ref[s], lens)
+    lens = lens[:, 0:1]
     live = [jnp.where(lens > t, 1.0, 0.0) for t in range(NEW)]
     big = NEW * SUB
     pr, pc = grid_of((big, block), 0), grid_of((big, block), 1)
@@ -291,6 +295,14 @@
     orow, ocol = grid_of((vcols, vcols), 0), grid_of((vcols, vcols), 1)
     part_n = vcols // GROUPS
     perm = one_hot(ocol == (orow & (part_n - 1)) * GROUPS + orow // part_n)
+    local = chans // HEAD_DIM
+    widen = one_hot(grid_of((local, chans), 0) == grid_of((local, chans), 1) // HEAD_DIM)
+    left = jnp.concatenate([bias_ref[...], rate_ref[...]], axis=0)
+    per_head = jnp.zeros((2 * LAYERS, chans), F32)
+    for _ in range(3):
+        piece = left.astype(BF)
+        per_head = per_head + dot(piece, widen)
+        left = left - piece.astype(F32)
     groups = GROUPS // n_tp
     per = chans // groups
     seq_of_row = grid_of((big, STATE), 0) & (SUB - 1)
@@ -302,6 +314,30 @@
         own = pltpu.make_async_copy(mine, wide.at[me_tp], own_sem.at[layer])
         own.start()
         own.wait()
+        if layer == 0:
+            vhs[...] = jnp.zeros_like(vhs)
+            chs[...] = jnp.zeros_like(chs)
+            for s in range(seqs):
+                for j in range(CONV - 1):
+                    row = SUB * j + s
+                    pair = vhist_ref[s, j].astype(F32)
+                    for l in range(LAYERS):
+                        vhs[l, row : row + 1, :] = pair[l : l + 1]
+                        both = chist_ref[l, s, j].astype(F32)
+                        chs[l, row : row + 1, :] = jnp.concatenate([both[0:1], both[1:2]], axis=1)
+            for l in range(LAYERS):
+                loads[l, "c"].wait()
+                cut = 64
+
+                def untangle(i, carry):
+                    at = pl.multiple_of(i * cut, cut)
+                    some = raw[l, pl.ds(at, cut)].astype(F32)
+                    cw[l, pl.ds(at, cut), :] = jnp.concatenate(
+                        [some[:, 0, :], some[:, 1, :]], axis=1
+                    ).astype(BF)
+                    return carry
+
+                lax.fori_loop(0, raw.shape[1] // cut, untangle, 0)
         for w in waits:
             w.wait_recv()
         for i in range(n_tp):
@@ -329,7 +365,6 @@
                 total = total + recv[layer, lax.rem(me_dp + n_dp - 1 - k, n_dp)].astype(F32)
             return total
 
-        loads[layer, "c"].wait()
         vec_part = dot(normed, cw[layer])
         loads[layer, "s"].wait()
         step_part = dot(normed, sw[layer])
@@ -348,9 +383,13 @@
         scaling = lax.rsqrt(total_sq / D + norm_floor)
         small = dot(spread, (sums[:, : vwide + heads_all] * scaling).astype(BF))
         conv, padded = conv_rows(
-            chist_ref[layer].astype(F32), small[:, :vwide], ctap_ref[layer]
-        )
-        nch_ref[layer] = keep_rows(padded, lens).astype(BF)
+            chs[layer], small[:, :vwide],
+            [
+                jnp.concatenate([ctap_ref[layer, k, 0:1], ctap_ref[layer, k, 1:2]], axis=1).astype(F32)
+                for k in range(CONV)
+            ],
+        )
+        nch_ref[layer] = keep_rows(padded, lens)
         conv = jnp.concatenate(conv, axis=0)
         stacked = jnp.concatenate(
             [conv[:, :vcols], conv[:, vcols:], jnp.zeros((128 - 2 * big, vcols), F32)], axis=0
@@ -365,24 +404,29 @@
         )
         recv_w[layer, me_tp] = send_w[layer, me_tp]
 
-        steps_wide = dot(expand_rows(small, vwide), expand) + bias_ref[layer : layer + 1]
+        steps_wide = dot(expand_rows(small, vwide), expand) + per_head[layer : layer + 1]
         steps_wide = softplus(steps_wide)
         step = [steps_wide[SUB * t : SUB * (t + 1)] * live[t] for t in range(NEW)]
-        rate = rate_ref[layer : layer + 1]
+        rate = per_head[LAYERS + layer : LAYERS + layer + 1]
         cum = [step[0] * rate]
         for t in range(1, NEW):
             cum.append(cum[-1] + step[t] * rate)
         values_in = dot(spread, (settle(waits_v, send_v, recv_v) * scaling).astype(BF))
-        value, padded = conv_rows(vhist_ref[layer].astype(F32), values_in, vtap_ref[layer])
-        nvh_ref[layer] = keep_rows(padded, lens).astype(BF)
+        value, padded = conv_rows(
+            vhs[layer], values_in, [vtap_ref[layer, k : k + 1].astype(F32) for k in range(CONV)]
+        )
+        nvh_ref[layer] = keep_rows(padded, lens)
         stepped = [step[t] * value[t] for t in range(NEW)]
         ending = [jnp.exp(cum[t] - cum[NEW - 1]) * stepped[t] for t in range(NEW)]
         gate_in = dot(spread, (settle(waits_g, send_g, recv_g) * scaling).astype(BF))
         gates = silu(gate_in)
+        fade = jnp.exp(-cum[NEW - 1])
+        fade_high = fade.astype(BF).astype(F32)
         zrows = jnp.concatenate(
-            ending + [jnp.exp(-cum[NEW - 1]), jnp.zeros((128 - big - SUB, chans), F32)], axis=0
-        )
-        zt_ref[layer] = zrows.T
+            ending + [fade_high, fade - fade_high, jnp.zeros((128 - big - 2 * SUB, chans), F32)],
+            axis=0,
+        )
+        zt_ref[layer] = zrows.T.astype(BF)
 
         for w in waits_w:
             w.wait_recv()
@@ -455,15 +499,41 @@
     return small[:, start:].astype(BF)
 
 
-def state_kernel(seqs, zt_ref, wr_ref, st_ref, out_ref):
+def state_kernel(
+    seqs, zt_ref, wr_ref, st_ref, fresh_ref, nvh_ref, nch_ref, out_ref, tok_ref, nv_ref, nc_ref
+):
     zt = zt_ref[0]
     big = NEW * SUB
-    weighted = zt[:, :big].astype(BF)
     write = wr_ref[0, 0].astype(F32)
-    seq_of_row = grid_of((big, STATE), 0) & (SUB - 1)
+    row = grid_of((big, STATE), 0)
+    rest = grid_of((128 - big, STATE), 0)
     for s in range(seqs):
-        picked = jnp.where(seq_of_row == s, write, 0.0).astype(BF)
-        out_ref[0, s] = zt[:, big + s : big + s + 1] * st_ref[0, s] + dot(weighted, picked)
+        picked = jnp.where((row & (SUB - 1)) == s, write, 0.0)
+        fading = jnp.where((rest == s) | (rest == SUB + s), 1.0, 0.0)
+        right = jnp.concatenate(
+            [
+                jnp.concatenate([picked, jnp.zeros((128 - big, STATE), F32)], axis=0),
+                jnp.concatenate([jnp.zeros((big, STATE), F32), fading], axis=0),
+            ],
+            axis=1,
+        ).astype(BF)
+        both = dot(zt, right)
+        out_ref[0, s] = both[:, STATE:] * st_ref[0, s] + both[:, :STATE]
+
+    @pl.when((pl.program_id(0) == 0) & (pl.program_id(1) == 0))
+    def _():
+        tok_ref[...] = fresh_ref[...]
+        half = nc_ref.shape[4]
+        for s in range(seqs):
+            for j in range(CONV - 1):
+                at = SUB * j + s
+                nv_ref[s, j] = jnp.concatenate(
+                    [nvh_ref[l, at : at + 1, :] for l in range(LAYERS)], axis=0
+                ).astype(BF)
+                for l in range(LAYERS):
+                    nc_ref[l, s, j] = jnp.concatenate(
+                        [nch_ref[l, at : at + 1, :half], nch_ref[l, at : at + 1, half:]], axis=0
+                    ).astype(BF)
 
 
 def fast_body(
@@ -477,13 +547,6 @@
     chans = value_weight.shape[2]
     vwide = 2 * vector_weight.shape[3]
     heads_all = step_weight.shape[2]
-    lens = jnp.broadcast_to(jnp.pad(lengths, (0, SUB - seqs))[:, None], (SUB, 128))
-    wide_bias = jnp.repeat(step_bias, HEAD_DIM, axis=1)
-    wide_rate = jnp.repeat(decay_rate, HEAD_DIM, axis=1)
-    pad = ((0, 0), (0, 0), (0, SUB - seqs), (0, 0))
-    vhist = jnp.pad(jnp.swapaxes(value_history, 1, 2), pad).reshape(LAYERS, -1, chans)
-    chist = vector_history.reshape(LAYERS, seqs, CONV - 1, vwide)
-    chist = jnp.pad(jnp.swapaxes(chist, 1, 2), pad).reshape(LAYERS, -1, vwide)
     state = recurrent_state.reshape(LAYERS, seqs, chans, STATE)
     groups = GROUPS // n_tp
     big = NEW * SUB
@@ -495,17 +558,20 @@
         functools.partial(step_kernel, n_tp, n_dp, (rows, seqs)),
         out_shape=(
             jax.ShapeDtypeStruct((rows, feats), BF),
-            jax.ShapeDtypeStruct((LAYERS, (CONV - 1) * SUB, chans), BF),
-            jax.ShapeDtypeStruct((LAYERS, (CONV - 1) * SUB, vwide), BF),
-            jax.ShapeDtypeStruct((LAYERS, chans, 128), F32),
+            jax.ShapeDtypeStruct((LAYERS, (CONV - 1) * SUB, chans), F32),
+            jax.ShapeDtypeStruct((LAYERS, (CONV - 1) * SUB, vwide), F32),
+            jax.ShapeDtypeStruct((LAYERS, chans, 128), BF),
             jax.ShapeDtypeStruct((LAYERS, groups, big, STATE), BF),
         ),
-        in_specs=[vm] * 9 + [hb] * 6,
+        in_specs=[vm, pl.BlockSpec(memory_space=pltpu.SMEM)] + [vm] * 7 + [hb] * 6,
         out_specs=(vm,) * 5,
         scratch_shapes=[
             pltpu.VMEM((LAYERS, feats, chans), BF),
             pltpu.VMEM((LAYERS, feats, chans), BF),
             pltpu.VMEM((LAYERS, feats, vwide), BF),
+            pltpu.VMEM((LAYERS, feats, 2, vwide // 2), BF),
+            pltpu.VMEM((LAYERS, (CONV - 1) * SUB, chans), F32),
+            pltpu.VMEM((LAYERS, (CONV - 1) * SUB, vwide), F32),
             pltpu.VMEM((LAYERS, feats, heads_all), BF),
             pltpu.VMEM((LAYERS, chans, feats), BF),
             pltpu.VMEM((LAYERS, seqs, chans, STATE), F32),
@@ -538,33 +604,47 @@
         ),
         name="step_kernel",
     )(
-        tokens, lens, norm_gain, wide_bias, wide_rate, value_taps.astype(F32),
-        vector_taps.reshape(LAYERS, CONV, vwide).astype(F32), vhist, chist,
-        gate_weight, value_weight, vector_weight.reshape(LAYERS, feats, vwide), step_weight,
+        tokens, lengths, norm_gain, step_bias, decay_rate, value_taps, vector_taps,
+        jnp.transpose(value_history, (1, 2, 0, 3)), vector_history,
+        gate_weight, value_weight, vector_weight, step_weight,
         out_weight, state,
     )
     cut = chans // groups // 2
-    next_state = pl.pallas_call(
+
+    def whole_block(shape):
+        return pl.BlockSpec(shape, lambda l, c: (0,) * len(shape))
+
+    turned = (seqs, CONV - 1, LAYERS, chans)
+    next_state, out, nv, nc = pl.pallas_call(
         functools.partial(state_kernel, seqs),
         grid=(LAYERS, chans // cut),
-        out_shape=jax.ShapeDtypeStruct(state.shape, F32),
+        out_shape=(
+            jax.ShapeDtypeStruct(state.shape, F32),
+            jax.ShapeDtypeStruct((rows, feats), BF),
+            jax.ShapeDtypeStruct(turned, BF),
+            jax.ShapeDtypeStruct(vector_history.shape, BF),
+        ),
         in_specs=[
             pl.BlockSpec((1, cut, 128), lambda l, c: (l, c, 0)),
             pl.BlockSpec((1, 1, big, STATE), lambda l, c: (l, c // 2, 0, 0)),
             pl.BlockSpec((1, seqs, cut, STATE), lambda l, c: (l, 0, c, 0)),
+            whole_block((rows, feats)),
+            whole_block(nvh.shape),
+            whole_block(nch.shape),
         ],
-        out_specs=pl.BlockSpec((1, seqs, cut, STATE), lambda l, c: (l, 0, c, 0)),
+        out_specs=(
+            pl.BlockSpec((1, seqs, cut, STATE), lambda l, c: (l, 0, c, 0)),
+            whole_block((rows, feats)),
+            whole_block(turned),
+            whole_block(vector_history.shape),
+        ),
         name="state_kernel",
-    )(zt, wr, state)
-
-    def unpack(rows_of, width):
-        return jnp.swapaxes(rows_of.reshape(LAYERS, CONV - 1, SUB, width)[:, :, :seqs], 1, 2)
-
+    )(zt, wr, state, fresh, nvh, nch)
     return (
-        fresh,
+        out,
         next_state.reshape(recurrent_state.shape),
-        unpack(nvh, chans),
-        unpack(nch, vwide).reshape(vector_history.shape),
+        jnp.transpose(nv, (2, 0, 1, 3)),
+        nc,
     )
 
 

time: 93.7 us -> 75.4 us (0.80)
  local copies, waits for them, and re-layouts: 16.6 us -> 0 us
  other arithmetic: 1.33 us -> 0 us
    reshape x7 -> x0, local copies, waits for them, and re-layouts: 7.07 us -> none  [the longest x1 4.37 us: fast_body(): vector_weight.reshape(LAYERS, feats, vwide)]
    unnamed x9 -> x0, local copies, waits for them, and re-layouts: 5.4 us -> none
    broadcast_in_dim x3 -> x0, local copies, waits for them, and re-layouts: 2.15 us -> none  [the longest x1 0.75 us: fast_body(): wide_bias = jnp.repeat(step_bias, HEAD_DIM, axis=1)]
    convert_element_type x1 -> x0, other arithmetic: 1.33 us -> none  [fast_body(): value_taps.astype(F32)]
    convert_element_type x1 -> x0, local copies, waits for them, and re-layouts: 1.31 us -> none  [fast_body(): vector_taps.reshape(LAYERS, CONV, vwide).astype(F32)]
where the time goes in v2:
time: 75.4 us; the launch traced here: 75.1 us
  Pallas kernels  74.5 us (99%)
    pallas_call x1, Pallas kernels, fast_body(): pl.pallas_call(functools.partial(step_kernel, n_tp, n_dp, (rows, seqs)),...  65 us
    pallas_call x1, Pallas kernels, fast_body(): pl.pallas_call(functools.partial(state_kernel, seqs), grid=(LAYERS, chans...  9.45 us

profile of v2, /device:TPU:0, one launch (start us, length us, event | category | flops | bytes accessed | tf_op | source)
XLA Modules:
  0.0 75.1 jit_solution(18373057467941166283)
XLA Ops:
  0.6 65.0 %step_kernel.1 = (bf16[12,1024]{1,0:T(8,128)(2,1)}, f32[2,24,1024]{2,1,0:T(8,128)}, f32[2,24,512]{2,1,0:T(8,128)}, bf16[2,1024,128]{2,1,0:T(8,128)(2,1)}, bf16[2,2,32,128]{3,2,1,0:T(8,128)(2,1)}) custom-call(bf16[12,1024]{1,0:T(8,128)(2,1)} %tok_ref.1, s32[6]{0:T(128)} %lens_ref.1, f32[2,1024]{1,0:T(2,128)} %gain_ref.1, f32[2,16]{1,0:T(2,128)} %bias_ref.1, ...), custom_call_target="tpu_custom_call" | custom-call | tf_op jit(solution)/shard_map/step_kernel/pallas_call | solution.py:557
  65.6 9.5 %state_kernel.1 = (f32[2,6,1024,128]{3,2,1,0:T(8,128)}, bf16[12,1024]{1,0:T(8,128)(2,1)}, bf16[6,3,2,1024]{3,2,1,0:T(2,128)(2,1)}, bf16[2,6,3,2,256]{4,3,2,1,0:T(2,128)(2,1)}) custom-call(bf16[2,1024,128]{2,1,0:T(8,128)(2,1)} %get-tuple-element.13.zt_ref, bf16[2,2,32,128]{3,2,1,0:T(8,128)(2,1)} %get-tuple-element.14.wr_ref, f32[2,6,1024,128]{3,2,1,0:T(8,128)} %bitcast.5, ...), custom_call_target="tpu_custom_call" | custom-call | tf_op jit(solution)/shard_map/state_kernel/pallas_call | solution.py:618

commit v3 on v2

--- a/solution.py
+++ b/solution.py
@@ -225,7 +225,7 @@
     tok_ref, lens_ref, gain_ref, bias_ref, rate_ref, vtap_ref, ctap_ref, vhist_ref, chist_ref,
     gw_hbm, vw_hbm, cw_hbm, sw_hbm, ow_hbm, st_hbm,
     out_ref, nvh_ref, nch_ref, zt_ref, wr_ref,
-    gw, vw, cw, raw, vhs, chs, sw, ow, st, whole, x32, tok, send_c, recv_c, send_v, recv_v, send_g, recv_g,
+    gw, vw, cw, raw, vhs, chs, sw, ow, st, stb, whole, x32, tok, send_c, recv_c, send_v, recv_v, send_g, recv_g,
     send_w, recv_w, send_m, recv_m, acc, send_o, recv_o,
     load_sem, own_sem, ag_s, ag_r, rs_s, rs_r, vx_s, vx_r, mx_s, mx_r, ox_s, ox_r,
 ):
@@ -325,19 +325,21 @@
                         vhs[l, row : row + 1, :] = pair[l : l + 1]
                         both = chist_ref[l, s, j].astype(F32)
                         chs[l, row : row + 1, :] = jnp.concatenate([both[0:1], both[1:2]], axis=1)
-            for l in range(LAYERS):
-                loads[l, "c"].wait()
-                cut = 64
-
-                def untangle(i, carry):
-                    at = pl.multiple_of(i * cut, cut)
-                    some = raw[l, pl.ds(at, cut)].astype(F32)
-                    cw[l, pl.ds(at, cut), :] = jnp.concatenate(
-                        [some[:, 0, :], some[:, 1, :]], axis=1
-                    ).astype(BF)
-                    return carry
-
-                lax.fori_loop(0, raw.shape[1] // cut, untangle, 0)
+        loads[layer, "c"].wait()
+        cut = 64
+
+        def untangle(i, carry):
+            at = pl.multiple_of(i * cut, cut)
+            some = raw[layer, pl.ds(at, cut)].astype(F32)
+            cw[layer, pl.ds(at, cut), :] = jnp.concatenate(
+                [some[:, 0, :], some[:, 1, :]], axis=1
+            ).astype(BF)
+            return carry
+
+        lax.fori_loop(0, raw.shape[1] // cut, untangle, 0)
+        loads[layer, "st"].wait()
+        for s in range(seqs):
+            stb[layer, s] = st[layer, s].astype(BF)
         for w in waits:
             w.wait_recv()
         for i in range(n_tp):
@@ -382,14 +384,13 @@
         total_sq = jnp.sum(sums[:, vwide + heads_all :], axis=1, keepdims=True)
         scaling = lax.rsqrt(total_sq / D + norm_floor)
         small = dot(spread, (sums[:, : vwide + heads_all] * scaling).astype(BF))
-        conv, padded = conv_rows(
+        conv, padded_vec = conv_rows(
             chs[layer], small[:, :vwide],
             [
                 jnp.concatenate([ctap_ref[layer, k, 0:1], ctap_ref[layer, k, 1:2]], axis=1).astype(F32)
                 for k in range(CONV)
             ],
         )
-        nch_ref[layer] = keep_rows(padded, lens)
         conv = jnp.concatenate(conv, axis=0)
         stacked = jnp.concatenate(
             [conv[:, :vcols], conv[:, vcols:], jnp.zeros((128 - 2 * big, vcols), F32)], axis=0
@@ -412,25 +413,18 @@
         for t in range(1, NEW):
             cum.append(cum[-1] + step[t] * rate)
         values_in = dot(spread, (settle(waits_v, send_v, recv_v) * scaling).astype(BF))
-        value, padded = conv_rows(
+        value, padded_val = conv_rows(
             vhs[layer], values_in, [vtap_ref[layer, k : k + 1].astype(F32) for k in range(CONV)]
         )
-        nvh_ref[layer] = keep_rows(padded, lens)
         stepped = [step[t] * value[t] for t in range(NEW)]
-        ending = [jnp.exp(cum[t] - cum[NEW - 1]) * stepped[t] for t in range(NEW)]
+        reach = [
+            [jnp.exp(cum[u] - cum[t]) * stepped[u] for u in range(t + 1)] for t in range(NEW)
+        ]
+        fades = [jnp.exp(-cum[t]) for t in range(NEW)]
         gate_in = dot(spread, (settle(waits_g, send_g, recv_g) * scaling).astype(BF))
         gates = silu(gate_in)
-        fade = jnp.exp(-cum[NEW - 1])
-        fade_high = fade.astype(BF).astype(F32)
-        zrows = jnp.concatenate(
-            ending + [fade_high, fade - fade_high, jnp.zeros((128 - big - 2 * SUB, chans), F32)],
-            axis=0,
-        )
-        zt_ref[layer] = zrows.T.astype(BF)
-
         for w in waits_w:
             w.wait_recv()
-        loads[layer, "st"].wait()
         half = each // groups
         y_parts = [[] for _ in range(NEW)]
         for g in range(groups):
@@ -445,18 +439,17 @@
             for s in range(seqs):
                 picked = jnp.where(seq_of_row == s, read, 0.0).astype(BF)
                 carried = carried + dot_nt(
-                    picked, st[layer, s, per * g : per * (g + 1), :].astype(BF)
+                    picked, stb[layer, s, per * g : per * (g + 1), :]
                 )
             span = slice(per * g, per * (g + 1))
             for t in range(NEW):
-                now = cum[t][:, span]
-                y = carried[SUB * t : SUB * (t + 1)] * jnp.exp(-now)
+                y = carried[SUB * t : SUB * (t + 1)] * fades[t][:, span]
                 for u in range(t + 1):
                     score = jnp.sum(
                         read[SUB * t : SUB * (t + 1)] * write[SUB * u : SUB * (u + 1)],
                         axis=1, keepdims=True,
                     )
-                    y = y + score * jnp.exp(cum[u][:, span] - now) * stepped[u][:, span]
+                    y = y + score * reach[t][u][:, span]
                 y_parts[t].append(y)
         mixed = jnp.concatenate(
             [
@@ -471,6 +464,15 @@
             mx_s.at[layer], mx_r.at[layer],
         )
         recv_m[layer, me_dp] = send_m[layer]
+        fade = fades[NEW - 1]
+        fade_high = fade.astype(BF).astype(F32)
+        zrows = jnp.concatenate(
+            reach[NEW - 1] + [fade_high, fade - fade_high, jnp.zeros((128 - big - 2 * SUB, chans), F32)],
+            axis=0,
+        )
+        zt_ref[layer] = zrows.T.astype(BF)
+        nch_ref[layer] = keep_rows(padded_vec, lens)
+        nvh_ref[layer] = keep_rows(padded_val, lens)
         for w in waits:
             w.wait_recv()
         loads[layer, "o"].wait()
@@ -500,40 +502,54 @@
 
 
 def state_kernel(
-    seqs, zt_ref, wr_ref, st_ref, fresh_ref, nvh_ref, nch_ref, out_ref, tok_ref, nv_ref, nc_ref
+    seqs, zt_ref, wr_ref, fresh_ref, nvh_ref, nch_ref, st_hbm, tok_ref, nv_ref, nc_ref, out_hbm,
+    old, new, in_sem, out_sem,
 ):
-    zt = zt_ref[0]
+    reads, writes = [], []
+    for l in range(LAYERS):
+        for s in range(seqs):
+            copy = pltpu.make_async_copy(st_hbm.at[l, s], old.at[l, s], in_sem.at[l, s])
+            copy.start()
+            reads.append(copy)
     big = NEW * SUB
-    write = wr_ref[0, 0].astype(F32)
     row = grid_of((big, STATE), 0)
     rest = grid_of((128 - big, STATE), 0)
+    groups = wr_ref.shape[1]
+    per = zt_ref.shape[1] // groups
+    tok_ref[...] = fresh_ref[...]
+    half = nc_ref.shape[4]
     for s in range(seqs):
-        picked = jnp.where((row & (SUB - 1)) == s, write, 0.0)
-        fading = jnp.where((rest == s) | (rest == SUB + s), 1.0, 0.0)
-        right = jnp.concatenate(
-            [
-                jnp.concatenate([picked, jnp.zeros((128 - big, STATE), F32)], axis=0),
-                jnp.concatenate([jnp.zeros((big, STATE), F32), fading], axis=0),
-            ],
-            axis=1,
-        ).astype(BF)
-        both = dot(zt, right)
-        out_ref[0, s] = both[:, STATE:] * st_ref[0, s] + both[:, :STATE]
-
-    @pl.when((pl.program_id(0) == 0) & (pl.program_id(1) == 0))
-    def _():
-        tok_ref[...] = fresh_ref[...]
-        half = nc_ref.shape[4]
+        for j in range(CONV - 1):
+            at = SUB * j + s
+            nv_ref[s, j] = jnp.concatenate(
+                [nvh_ref[l, at : at + 1, :] for l in range(LAYERS)], axis=0
+            ).astype(BF)
+            for l in range(LAYERS):
+                nc_ref[l, s, j] = jnp.concatenate(
+                    [nch_ref[l, at : at + 1, :half], nch_ref[l, at : at + 1, half:]], axis=0
+                ).astype(BF)
+    for l in range(LAYERS):
         for s in range(seqs):
-            for j in range(CONV - 1):
-                at = SUB * j + s
-                nv_ref[s, j] = jnp.concatenate(
-                    [nvh_ref[l, at : at + 1, :] for l in range(LAYERS)], axis=0
+            reads[l * seqs + s].wait()
+            fading = jnp.where((rest == s) | (rest == SUB + s), 1.0, 0.0)
+            for g in range(groups):
+                write = wr_ref[l, g].astype(F32)
+                picked = jnp.where((row & (SUB - 1)) == s, write, 0.0)
+                right = jnp.concatenate(
+                    [
+                        jnp.concatenate([picked, jnp.zeros((128 - big, STATE), F32)], axis=0),
+                        jnp.concatenate([jnp.zeros((big, STATE), F32), fading], axis=0),
+                    ],
+                    axis=1,
                 ).astype(BF)
-                for l in range(LAYERS):
-                    nc_ref[l, s, j] = jnp.concatenate(
-                        [nch_ref[l, at : at + 1, :half], nch_ref[l, at : at + 1, half:]], axis=0
-                    ).astype(BF)
+                span = slice(per * g, per * (g + 1))
+                both = dot(zt_ref[l, span, :], right)
+                new[l, s, span, :] = both[:, STATE:] * old[l, s, span, :] + both[:, :STATE]
+            copy = pltpu.make_async_copy(new.at[l, s], out_hbm.at[l, s], out_sem.at[l, s])
+            copy.start()
+            writes.append(copy)
+    for copy in writes:
+        copy.wait()
 
 
 def fast_body(
@@ -575,6 +591,7 @@
             pltpu.VMEM((LAYERS, feats, heads_all), BF),
             pltpu.VMEM((LAYERS, chans, feats), BF),
             pltpu.VMEM((LAYERS, seqs, chans, STATE), F32),
+            pltpu.VMEM((LAYERS, seqs, chans, STATE), BF),
             pltpu.VMEM((LAYERS, n_tp, rows, feats), BF),
             pltpu.VMEM((n_tp * rows, feats), F32),
             pltpu.VMEM((rows, feats), BF),
@@ -609,37 +626,25 @@
         gate_weight, value_weight, vector_weight, step_weight,
         out_weight, state,
     )
-    cut = chans // groups // 2
-
-    def whole_block(shape):
-        return pl.BlockSpec(shape, lambda l, c: (0,) * len(shape))
-
     turned = (seqs, CONV - 1, LAYERS, chans)
-    next_state, out, nv, nc = pl.pallas_call(
+    out, nv, nc, next_state = pl.pallas_call(
         functools.partial(state_kernel, seqs),
-        grid=(LAYERS, chans // cut),
         out_shape=(
-            jax.ShapeDtypeStruct(state.shape, F32),
             jax.ShapeDtypeStruct((rows, feats), BF),
             jax.ShapeDtypeStruct(turned, BF),
             jax.ShapeDtypeStruct(vector_history.shape, BF),
+            jax.ShapeDtypeStruct(state.shape, F32),
         ),
-        in_specs=[
-            pl.BlockSpec((1, cut, 128), lambda l, c: (l, c, 0)),
-            pl.BlockSpec((1, 1, big, STATE), lambda l, c: (l, c // 2, 0, 0)),
-            pl.BlockSpec((1, seqs, cut, STATE), lambda l, c: (l, 0, c, 0)),
-            whole_block((rows, feats)),
-            whole_block(nvh.shape),
-            whole_block(nch.shape),
+        in_specs=[vm] * 5 + [hb],
+        out_specs=(vm, vm, vm, hb),
+        scratch_shapes=[
+            pltpu.VMEM(state.shape, F32),
+            pltpu.VMEM(state.shape, F32),
+            dma((LAYERS, seqs)),
+            dma((LAYERS, seqs)),
         ],
-        out_specs=(
-            pl.BlockSpec((1, seqs, cut, STATE), lambda l, c: (l, 0, c, 0)),
-            whole_block((rows, feats)),
-            whole_block(turned),
-            whole_block(vector_history.shape),
-        ),
         name="state_kernel",
-    )(zt, wr, state, fresh, nvh, nch)
+    )(zt, wr, fresh, nvh, nch, state)
     return (
         out,
         next_state.reshape(recurrent_state.shape),

time: 75.4 us -> 72.9 us (0.967)
  Pallas kernels: 74.5 us -> 72.1 us
    pallas_call x1, Pallas kernels: 9.45 us -> 7.17 us  [fast_body(): pl.pallas_call(functools.partial(state_kernel, seqs), out_shape=(jax.Shap...]
where the time goes in v3:
time: 72.9 us; the launch traced here: 72.8 us
  Pallas kernels  72.1 us (99%)
    pallas_call x1, Pallas kernels, fast_body(): pl.pallas_call(functools.partial(step_kernel, n_tp, n_dp, (rows, seqs)),...  64.9 us
    pallas_call x1, Pallas kernels, fast_body(): pl.pallas_call(functools.partial(state_kernel, seqs), out_shape=(jax.Shap...  7.17 us

profile of v3, /device:TPU:0, one launch (start us, length us, event | category | flops | bytes accessed | tf_op | source)
XLA Modules:
  0.0 72.8 jit_solution(1101409807630299217)
XLA Ops:
  0.6 64.9 %step_kernel.1 = (bf16[12,1024]{1,0:T(8,128)(2,1)}, f32[2,24,1024]{2,1,0:T(8,128)}, f32[2,24,512]{2,1,0:T(8,128)}, bf16[2,1024,128]{2,1,0:T(8,128)(2,1)}, bf16[2,2,32,128]{3,2,1,0:T(8,128)(2,1)}) custom-call(bf16[12,1024]{1,0:T(8,128)(2,1)} %tok_ref.1, s32[6]{0:T(128)} %lens_ref.1, f32[2,1024]{1,0:T(2,128)} %gain_ref.1, f32[2,16]{1,0:T(2,128)} %bias_ref.1, ...), custom_call_target="tpu_custom_call" | custom-call | tf_op jit(solution)/shard_map/step_kernel/pallas_call | solution.py:573
  65.6 7.2 %state_kernel.1 = (bf16[12,1024]{1,0:T(8,128)(2,1)}, bf16[6,3,2,1024]{3,2,1,0:T(2,128)(2,1)}, bf16[2,6,3,2,256]{4,3,2,1,0:T(2,128)(2,1)}, f32[2,6,1024,128]{3,2,1,0:T(8,128)}) custom-call(bf16[2,1024,128]{2,1,0:T(8,128)(2,1)} %get-tuple-element.13.zt_ref, bf16[2,2,32,128]{3,2,1,0:T(8,128)(2,1)} %get-tuple-element.14.wr_ref, ...), custom_call_target="tpu_custom_call" | custom-call | tf_op jit(solution)/shard_map/state_kernel/pallas_call | solution.py:630
